TPU v7x, 128 devices: a whole 4x4x4 slice. The times are simulated.
128 devices in a mesh: sp: 32 (over z, y, core), tp: 4 (over x).
Axes of the slice: x: 4, y: 4, z: 4, core: 2. Of those that a mesh axis runs over, the one named last changes fastest.
Arguments:
- tokens: bfloat16 [16384, 2048], P(('sp', 'tp')), may hold values from -6 to 6
- norm_gain: float32 [2048], replicated, may hold values from 0.1 to 1.9
- query_weight: bfloat16 [2048, 1024], P(None, 'tp'), may hold values from -0.13258252 to 0.13258252
- key_weight: bfloat16 [2048, 1024], P(None, 'tp'), may hold values from -0.13258252 to 0.13258252
- value_weight: bfloat16 [2048, 1024], P(None, 'tp'), may hold values from -0.125 to 0.125
- glu_value_weight: bfloat16 [2048, 1024], P(None, 'tp'), may hold values from -0.125 to 0.125
- glu_gate_weight: bfloat16 [2048, 1024], P(None, 'tp'), may hold values from -0.125 to 0.125
- qk_gain: float32 [2, 64], replicated, may hold values from 1 to 6
- mix_lambda: float32 [8], P('tp'), may hold values from 0.3 to 0.8
- head_gain: float32 [128], replicated, may hold values from 0.1 to 1.9
- conv_kernel: float32 [31, 1024], P(None, 'tp'), may hold values from -1 to 1
- channel_gain: float32 [1024], P('tp'), may hold values from 0.1 to 1.9
- channel_shift: float32 [1024], P('tp'), may hold values from -3 to 3
- output_weight: bfloat16 [2048, 2048], replicated, may hold values from -0.125 to 0.125
Outputs:
- mixed: bfloat16 [16384, 2048], P(('sp', 'tp'))
- log_totals: float32 [2, 8, 16384], P(None, 'tp', 'sp')
All inputs are finite; a program needn't handle non-finite values.
Results may differ from a plain program's by a relative error of at most 0.035.
Values may be sent and summed in bfloat16 or wider, within the bound.
A program may use at most 128 MiB of HBM per device.

v0:
```python
import math
import jax
import jax.numpy as jnp
from jax import lax
from jax.sharding import PartitionSpec as P


def joined_along(tiles, dim):
    dims = list(tiles.shape[1:])
    dims[dim] *= tiles.shape[0]
    return jnp.moveaxis(tiles, 0, dim).reshape(dims)


def sent_to_all(shard, axis):
    copies = jnp.broadcast_to(shard, (lax.axis_size(axis), *shard.shape))
    return lax.all_to_all(copies, axis, split_axis=0, concat_axis=0, tiled=True)


def collect(shard, axis, dim):
    return joined_along(sent_to_all(shard, axis), dim)


def from_behind(value, axis, steps):
    count = lax.axis_size(axis)
    leading, last = (max(0, -steps), min(count, count - steps))
    return lax.ppermute(value, axis, [(source, source + steps) for source in range(leading, last)])


def over_copies(shard, axis):
    everything = sent_to_all(shard, axis)
    return jnp.sum(everything, axis=0)


def in_one(arrays, axis):
    ends = [0]
    for a in arrays:
        ends.append(ends[-1] + a.size)
    total = over_copies(jnp.concatenate([a.ravel() for a in arrays]), axis)
    return tuple((total[b:e].reshape(a.shape) for a, b, e in zip(arrays, ends, ends[1:])))


def rotate(values, positions):
    half = values.shape[-1] // 2
    inverse = 10000.0 ** (-jnp.arange(0, half, dtype=jnp.float32) * 2.0 / values.shape[-1])
    angles = positions[:, None] * inverse[None, :]
    cosine = jnp.cos(angles)[:, None, None, :]
    sine = jnp.sin(angles)[:, None, None, :]
    first = values[..., :half]
    second = values[..., half:]
    return jnp.concatenate(
        [first * cosine - second * sine, second * cosine + first * sine], axis=-1
    )


def prepare(raw, qk_gain, positions):
    values = raw.astype(jnp.float32)
    values = values * lax.rsqrt(jnp.mean(values * values, axis=-1, keepdims=True) + 1e-06)
    values = values * qk_gain[None, None, :, :]
    return rotate(values, positions).astype(jnp.bfloat16)


def per_device(
    tokens,
    norm_gain,
    query_weight,
    key_weight,
    value_weight,
    glu_value_weight,
    glu_gate_weight,
    qk_gain,
    mix_lambda,
    head_gain,
    conv_kernel,
    channel_gain,
    channel_shift,
    output_weight,
):
    head_size = qk_gain.shape[1]
    heads_here = mix_lambda.shape[0]
    value_size = head_gain.shape[0]
    kernel_len = conv_kernel.shape[0]
    conv_here = conv_kernel.shape[1]
    width = tokens.shape[1]
    matrices = (query_weight, key_weight, value_weight, glu_value_weight, glu_gate_weight)

    def project(piece):
        inputs = piece.astype(jnp.float32)
        normed = (
            inputs
            * lax.rsqrt(jnp.mean(inputs * inputs, axis=-1, keepdims=True) + 1e-06)
            * norm_gain
        ).astype(jnp.bfloat16)
        results = [
            jnp.dot(normed, matrix, preferred_element_type=jnp.float32).astype(jnp.bfloat16)
            for matrix in matrices
        ]
        return jnp.concatenate(results, axis=1)

    projected = project(collect(tokens, "tp", 0))
    tok_rows = projected.shape[0]
    bounds = [0]
    for matrix in matrices:
        bounds.append(bounds[-1] + matrix.shape[1])
    queries = projected[:, bounds[0] : bounds[1]].reshape(tok_rows, heads_here, 2, head_size)
    keys = projected[:, bounds[1] : bounds[2]].reshape(tok_rows, heads_here, 2, head_size)
    values = projected[:, bounds[2] : bounds[3]].reshape(tok_rows, heads_here, value_size)
    glu_a = projected[:, bounds[3] : bounds[4]]
    glu_g = projected[:, bounds[4] : bounds[5]]
    offset = lax.axis_index("sp") * tok_rows
    query_pos = offset + jnp.arange(tok_rows, dtype=jnp.int32)
    float_pos = query_pos.astype(jnp.float32)
    rq = jnp.transpose(prepare(queries, qk_gain, float_pos), (1, 2, 0, 3))
    rk = prepare(keys, qk_gain, float_pos)
    scale = head_size ** (-0.5)
    last_query = offset + tok_rows - 1
    initial = (
        jnp.full((heads_here, 2, tok_rows), -1e30, jnp.float32),
        jnp.zeros((heads_here, 2, tok_rows), jnp.float32),
        jnp.zeros((heads_here, 2, tok_rows, value_size), jnp.float32),
    )
    carry = initial
    key_piece = lax.all_gather(rk, "sp", axis=0, tiled=True)
    value_piece = lax.all_gather(values, "sp", axis=0, tiled=True)
    count = key_piece.shape[0]
    block = math.gcd(count, 512)
    blocks = count // block
    key_blocks = key_piece.reshape(blocks, block, heads_here, 2, head_size)
    value_blocks = value_piece.reshape(blocks, block, heads_here, value_size)

    def advance(state, item):
        key_block, value_block, number = item
        key_start = number * block

        def compute(inner):
            running, totals, summed = inner
            scores = (
                jnp.einsum("hmqd,khmd->hmqk", rq, key_block, preferred_element_type=jnp.float32)
                * scale
            )
            key_pos = key_start + jnp.arange(block, dtype=jnp.int32)
            allowed = key_pos[None, :] <= query_pos[:, None]
            scores = jnp.where(allowed[None, None], scores, -1e30)
            newtop = jnp.maximum(running, jnp.max(scores, axis=-1))
            probs = jnp.where(allowed[None, None], jnp.exp(scores - newtop[..., None]), 0.0)
            factor = jnp.exp(running - newtop)
            totals = totals * factor + jnp.sum(probs, axis=-1)
            added = jnp.einsum(
                "hmqk,khd->hmqd",
                probs.astype(jnp.bfloat16),
                value_block,
                preferred_element_type=jnp.float32,
            )
            return (newtop, totals, summed * factor[..., None] + added)

        def keep(inner):
            return inner

        return (lax.cond(key_start <= last_query, compute, keep, state), None)

    carry, unused = lax.scan(
        advance, carry, (key_blocks, value_blocks, jnp.arange(blocks, dtype=jnp.int32))
    )
    running, totals, summed = carry
    heads_out = (
        summed[:, 0] / totals[:, 0, :, None]
        - mix_lambda[:, None, None] * summed[:, 1] / totals[:, 1, :, None]
    )
    heads_out = (
        heads_out
        * lax.rsqrt(jnp.mean(heads_out * heads_out, axis=-1, keepdims=True) + 1e-06)
        * head_gain
    )
    attended = jnp.transpose(heads_out.astype(jnp.bfloat16), (1, 0, 2)).reshape(
        tok_rows, heads_here * value_size
    )
    log_totals = jnp.transpose(running + jnp.log(totals), (1, 0, 2))
    gated = (glu_a.astype(jnp.float32) * jax.nn.sigmoid(glu_g.astype(jnp.float32))).astype(
        jnp.bfloat16
    )
    earlier = from_behind(gated[tok_rows - (kernel_len - 1) :], "sp", 1)
    extended = jnp.concatenate([earlier, gated], axis=0).astype(jnp.float32)
    convolved = jnp.zeros((tok_rows, conv_here), jnp.float32)
    for step in range(kernel_len):
        convolved = convolved + conv_kernel[step][None, :] * extended[step : step + tok_rows]
    plain_sum, square_sum = in_one(
        (jnp.sum(convolved, axis=1), jnp.sum(convolved * convolved, axis=1)), "tp"
    )
    channels = conv_here * lax.axis_size("tp")
    middle = (plain_sum / channels)[:, None]
    spread = (square_sum / channels)[:, None] - middle * middle
    conv_out = jax.nn.silu(
        (convolved - middle) * lax.rsqrt(spread + 1e-05) * channel_gain + channel_shift
    ).astype(jnp.bfloat16)
    merged = jnp.concatenate([attended, conv_out], axis=1)
    groups = lax.axis_size("tp")
    branch_width = heads_here * value_size
    weight_view = output_weight.reshape(2, groups, branch_width, width)
    moved = lax.all_to_all(merged, "tp", split_axis=0, concat_axis=1, tiled=True)
    arranged = moved.reshape(tok_rows // groups, groups, 2, branch_width)
    mixed = jnp.einsum(
        "rtcj,ctjd->rd", arranged, weight_view, preferred_element_type=jnp.float32
    ).astype(jnp.bfloat16)
    return (mixed, log_totals)


def solution(mesh):
    placed = (
        P(("sp", "tp"), None),
        P(),
        P(None, "tp"),
        P(None, "tp"),
        P(None, "tp"),
        P(None, "tp"),
        P(None, "tp"),
        P(),
        P("tp"),
        P(),
        P(None, "tp"),
        P("tp"),
        P("tp"),
        P(),
    )
    return jax.shard_map(
        per_device,
        mesh=mesh,
        in_specs=placed,
        out_specs=(P(("sp", "tp"), None), P(None, "tp", "sp")),
        check_vma=False,
    )
```

profile of v0, /device:TPU:121, one launch (start us, length us, event | category | flops | bytes accessed | tf_op | source)
XLA Modules:
  0.0 416.1 jit_solution(1099823068784679302)
XLA Ops:
  14.3 25.1 %all-to-all-done = bf16[4,128,2048]{2,1,0:T(8,128)(2,1)S(1)} async-done(((bf16[4,128,2048]{2,1,0:T(8,128)(2,1)}), bf16[4,128,2048]{2,1,0:T(8,128)(2,1)S(1)}, u32[]{:S(2)}, u32[]{:S(2)}) %all-to-all-start) | async-done | bytes 2097184 | tf_op jit(solution)/shard_map/all_to_all | solution.py:16
  65.8 35.1 %all-gather.3.cloned.1.call-done = bf16[16384,2,2,64]{0,3,2,1:T(8,128)(2,1)} async-done(((bf16[512,2,2,64]{0,3,2,1:T(8,128)(2,1)}), bf16[16384,2,2,64]{0,3,2,1:T(8,128)(2,1)}) %all-gather.3.cloned.1.call-update) | async-done | bytes 8388624 | tf_op jit(solution)/shard_map/all_gather | solution.py:122
  100.9 7.9 %copy.75 = bf16[2,2,8,32,8,512]{5,4,2,1,0,3:T(8,128)(2,1)} copy(bf16[2,2,8,32,8,512]{5,4,3,2,1,0:T(8,128)(2,1)} %bitcast.129) | data formatting | bytes 16777216 | tf_op jit(solution)/shard_map/reshape | solution.py:127
  108.8 46.9 %all-gather.5.cloned.1.call-done = bf16[16384,2,128]{2,0,1:T(8,128)(2,1)} async-done(((bf16[512,2,128]{2,0,1:T(8,128)(2,1)}), bf16[16384,2,128]{2,0,1:T(8,128)(2,1)}) %all-gather.5.cloned.1.call-update) | async-done | bytes 8388624 | tf_op jit(solution)/shard_map/all_gather | solution.py:123
  155.6 7.6 %copy.43 = bf16[32,512,2,128]{3,1,2,0:T(8,128)(2,1)} copy(bf16[32,512,2,128]{3,1,0,2:T(8,128)(2,1)} %bitcast.130) | data formatting | bytes 16777216
  163.4 227.0 %while.15 = (s32[]{:T(128)}, f32[2,2,512]{2,1,0:T(2,128)S(1)}, f32[2,2,512]{2,1,0:T(2,128)S(1)}, f32[2,2,512,128]{3,2,1,0:T(8,128)S(1)}, s32[32]{0:T(128)S(1)}, ...) while((s32[]{:T(128)}, f32[2,2,512]{2,1,0:T(2,128)S(1)}, ...), condition=%wide.region_8.9_spmd.clone, body=%wide.region_3.8_spmd.clone.sunk | while | flops 417076224 | bytes 16659763 | solution.py:160
  171.6 5.9 %conditional.3 = ((f32[2,2,512]{2,1,0:T(2,128)S(1)}, f32[2,2,512]{2,1,0:T(2,128)S(1)}, f32[2,2,512,128]{3,2,1,0:T(8,128)S(1)})) conditional(s32[]{:T(128)} %convert_element_type.153, (f32[2,2,512]{2,1,0:T(2,128)S(1)}, f32[2,2,512]{2,1,0:T(2,128)S(1)}, f32[2,2,512,128]{3,2,1,0:T(8,128)S(1)}) %tuple.89, (s32[]{:T(128)}, s32[]{:T(128)}, ...), branch_computations={%region_4.4_spmd, %region_5.7_spmd} | conditional | flops 417076224 | bytes 16657448 | solution.py:158
  185.8 5.9 %conditional.3 = ((f32[2,2,512]{2,1,0:T(2,128)S(1)}, f32[2,2,512]{2,1,0:T(2,128)S(1)}, f32[2,2,512,128]{3,2,1,0:T(8,128)S(1)})) conditional(s32[]{:T(128)} %convert_element_type.153, (f32[2,2,512]{2,1,0:T(2,128)S(1)}, f32[2,2,512]{2,1,0:T(2,128)S(1)}, f32[2,2,512,128]{3,2,1,0:T(8,128)S(1)}) %tuple.89, (s32[]{:T(128)}, s32[]{:T(128)}, ...), branch_computations={%region_4.4_spmd, %region_5.7_spmd} | conditional | flops 417076224 | bytes 16657448 | solution.py:158
  200.0 5.9 %conditional.3 = ((f32[2,2,512]{2,1,0:T(2,128)S(1)}, f32[2,2,512]{2,1,0:T(2,128)S(1)}, f32[2,2,512,128]{3,2,1,0:T(8,128)S(1)})) conditional(s32[]{:T(128)} %convert_element_type.153, (f32[2,2,512]{2,1,0:T(2,128)S(1)}, f32[2,2,512]{2,1,0:T(2,128)S(1)}, f32[2,2,512,128]{3,2,1,0:T(8,128)S(1)}) %tuple.89, (s32[]{:T(128)}, s32[]{:T(128)}, ...), branch_computations={%region_4.4_spmd, %region_5.7_spmd} | conditional | flops 417076224 | bytes 16657448 | solution.py:158
  207.1 5.9 %conditional.3 = ((f32[2,2,512]{2,1,0:T(2,128)S(1)}, f32[2,2,512]{2,1,0:T(2,128)S(1)}, f32[2,2,512,128]{3,2,1,0:T(8,128)S(1)})) conditional(s32[]{:T(128)} %convert_element_type.153, (f32[2,2,512]{2,1,0:T(2,128)S(1)}, f32[2,2,512]{2,1,0:T(2,128)S(1)}, f32[2,2,512,128]{3,2,1,0:T(8,128)S(1)}) %tuple.89, (s32[]{:T(128)}, s32[]{:T(128)}, ...), branch_computations={%region_4.4_spmd, %region_5.7_spmd} | conditional | flops 417076224 | bytes 16657448 | solution.py:158
  214.2 5.9 %conditional.3 = ((f32[2,2,512]{2,1,0:T(2,128)S(1)}, f32[2,2,512]{2,1,0:T(2,128)S(1)}, f32[2,2,512,128]{3,2,1,0:T(8,128)S(1)})) conditional(s32[]{:T(128)} %convert_element_type.153, (f32[2,2,512]{2,1,0:T(2,128)S(1)}, f32[2,2,512]{2,1,0:T(2,128)S(1)}, f32[2,2,512,128]{3,2,1,0:T(8,128)S(1)}) %tuple.89, (s32[]{:T(128)}, s32[]{:T(128)}, ...), branch_computations={%region_4.4_spmd, %region_5.7_spmd} | conditional | flops 417076224 | bytes 16657448 | solution.py:158
  228.4 5.9 %conditional.3 = ((f32[2,2,512]{2,1,0:T(2,128)S(1)}, f32[2,2,512]{2,1,0:T(2,128)S(1)}, f32[2,2,512,128]{3,2,1,0:T(8,128)S(1)})) conditional(s32[]{:T(128)} %convert_element_type.153, (f32[2,2,512]{2,1,0:T(2,128)S(1)}, f32[2,2,512]{2,1,0:T(2,128)S(1)}, f32[2,2,512,128]{3,2,1,0:T(8,128)S(1)}) %tuple.89, (s32[]{:T(128)}, s32[]{:T(128)}, ...), branch_computations={%region_4.4_spmd, %region_5.7_spmd} | conditional | flops 417076224 | bytes 16657448 | solution.py:158
  242.6 5.9 %conditional.3 = ((f32[2,2,512]{2,1,0:T(2,128)S(1)}, f32[2,2,512]{2,1,0:T(2,128)S(1)}, f32[2,2,512,128]{3,2,1,0:T(8,128)S(1)})) conditional(s32[]{:T(128)} %convert_element_type.153, (f32[2,2,512]{2,1,0:T(2,128)S(1)}, f32[2,2,512]{2,1,0:T(2,128)S(1)}, f32[2,2,512,128]{3,2,1,0:T(8,128)S(1)}) %tuple.89, (s32[]{:T(128)}, s32[]{:T(128)}, ...), branch_computations={%region_4.4_spmd, %region_5.7_spmd} | conditional | flops 417076224 | bytes 16657448 | solution.py:158
  256.7 5.9 %conditional.3 = ((f32[2,2,512]{2,1,0:T(2,128)S(1)}, f32[2,2,512]{2,1,0:T(2,128)S(1)}, f32[2,2,512,128]{3,2,1,0:T(8,128)S(1)})) conditional(s32[]{:T(128)} %convert_element_type.153, (f32[2,2,512]{2,1,0:T(2,128)S(1)}, f32[2,2,512]{2,1,0:T(2,128)S(1)}, f32[2,2,512,128]{3,2,1,0:T(8,128)S(1)}) %tuple.89, (s32[]{:T(128)}, s32[]{:T(128)}, ...), branch_computations={%region_4.4_spmd, %region_5.7_spmd} | conditional | flops 417076224 | bytes 16657448 | solution.py:158
  270.9 5.9 %conditional.3 = ((f32[2,2,512]{2,1,0:T(2,128)S(1)}, f32[2,2,512]{2,1,0:T(2,128)S(1)}, f32[2,2,512,128]{3,2,1,0:T(8,128)S(1)})) conditional(s32[]{:T(128)} %convert_element_type.153, (f32[2,2,512]{2,1,0:T(2,128)S(1)}, f32[2,2,512]{2,1,0:T(2,128)S(1)}, f32[2,2,512,128]{3,2,1,0:T(8,128)S(1)}) %tuple.89, (s32[]{:T(128)}, s32[]{:T(128)}, ...), branch_computations={%region_4.4_spmd, %region_5.7_spmd} | conditional | flops 417076224 | bytes 16657448 | solution.py:158
  285.1 5.9 %conditional.3 = ((f32[2,2,512]{2,1,0:T(2,128)S(1)}, f32[2,2,512]{2,1,0:T(2,128)S(1)}, f32[2,2,512,128]{3,2,1,0:T(8,128)S(1)})) conditional(s32[]{:T(128)} %convert_element_type.153, (f32[2,2,512]{2,1,0:T(2,128)S(1)}, f32[2,2,512]{2,1,0:T(2,128)S(1)}, f32[2,2,512,128]{3,2,1,0:T(8,128)S(1)}) %tuple.89, (s32[]{:T(128)}, s32[]{:T(128)}, ...), branch_computations={%region_4.4_spmd, %region_5.7_spmd} | conditional | flops 417076224 | bytes 16657448 | solution.py:158
  299.3 5.9 %conditional.3 = ((f32[2,2,512]{2,1,0:T(2,128)S(1)}, f32[2,2,512]{2,1,0:T(2,128)S(1)}, f32[2,2,512,128]{3,2,1,0:T(8,128)S(1)})) conditional(s32[]{:T(128)} %convert_element_type.153, (f32[2,2,512]{2,1,0:T(2,128)S(1)}, f32[2,2,512]{2,1,0:T(2,128)S(1)}, f32[2,2,512,128]{3,2,1,0:T(8,128)S(1)}) %tuple.89, (s32[]{:T(128)}, s32[]{:T(128)}, ...), branch_computations={%region_4.4_spmd, %region_5.7_spmd} | conditional | flops 417076224 | bytes 16657448 | solution.py:158
  313.5 5.9 %conditional.3 = ((f32[2,2,512]{2,1,0:T(2,128)S(1)}, f32[2,2,512]{2,1,0:T(2,128)S(1)}, f32[2,2,512,128]{3,2,1,0:T(8,128)S(1)})) conditional(s32[]{:T(128)} %convert_element_type.153, (f32[2,2,512]{2,1,0:T(2,128)S(1)}, f32[2,2,512]{2,1,0:T(2,128)S(1)}, f32[2,2,512,128]{3,2,1,0:T(8,128)S(1)}) %tuple.89, (s32[]{:T(128)}, s32[]{:T(128)}, ...), branch_computations={%region_4.4_spmd, %region_5.7_spmd} | conditional | flops 417076224 | bytes 16657448 | solution.py:158
  327.7 5.9 %conditional.3 = ((f32[2,2,512]{2,1,0:T(2,128)S(1)}, f32[2,2,512]{2,1,0:T(2,128)S(1)}, f32[2,2,512,128]{3,2,1,0:T(8,128)S(1)})) conditional(s32[]{:T(128)} %convert_element_type.153, (f32[2,2,512]{2,1,0:T(2,128)S(1)}, f32[2,2,512]{2,1,0:T(2,128)S(1)}, f32[2,2,512,128]{3,2,1,0:T(8,128)S(1)}) %tuple.89, (s32[]{:T(128)}, s32[]{:T(128)}, ...), branch_computations={%region_4.4_spmd, %region_5.7_spmd} | conditional | flops 417076224 | bytes 16657448 | solution.py:158
  341.9 5.9 %conditional.3 = ((f32[2,2,512]{2,1,0:T(2,128)S(1)}, f32[2,2,512]{2,1,0:T(2,128)S(1)}, f32[2,2,512,128]{3,2,1,0:T(8,128)S(1)})) conditional(s32[]{:T(128)} %convert_element_type.153, (f32[2,2,512]{2,1,0:T(2,128)S(1)}, f32[2,2,512]{2,1,0:T(2,128)S(1)}, f32[2,2,512,128]{3,2,1,0:T(8,128)S(1)}) %tuple.89, (s32[]{:T(128)}, s32[]{:T(128)}, ...), branch_computations={%region_4.4_spmd, %region_5.7_spmd} | conditional | flops 417076224 | bytes 16657448 | solution.py:158
  356.1 5.9 %conditional.3 = ((f32[2,2,512]{2,1,0:T(2,128)S(1)}, f32[2,2,512]{2,1,0:T(2,128)S(1)}, f32[2,2,512,128]{3,2,1,0:T(8,128)S(1)})) conditional(s32[]{:T(128)} %convert_element_type.153, (f32[2,2,512]{2,1,0:T(2,128)S(1)}, f32[2,2,512]{2,1,0:T(2,128)S(1)}, f32[2,2,512,128]{3,2,1,0:T(8,128)S(1)}) %tuple.89, (s32[]{:T(128)}, s32[]{:T(128)}, ...), branch_computations={%region_4.4_spmd, %region_5.7_spmd} | conditional | flops 417076224 | bytes 16657448 | solution.py:158
  370.3 5.9 %conditional.3 = ((f32[2,2,512]{2,1,0:T(2,128)S(1)}, f32[2,2,512]{2,1,0:T(2,128)S(1)}, f32[2,2,512,128]{3,2,1,0:T(8,128)S(1)})) conditional(s32[]{:T(128)} %convert_element_type.153, (f32[2,2,512]{2,1,0:T(2,128)S(1)}, f32[2,2,512]{2,1,0:T(2,128)S(1)}, f32[2,2,512,128]{3,2,1,0:T(8,128)S(1)}) %tuple.89, (s32[]{:T(128)}, s32[]{:T(128)}, ...), branch_computations={%region_4.4_spmd, %region_5.7_spmd} | conditional | flops 417076224 | bytes 16657448 | solution.py:158
  384.5 5.9 %conditional.3 = ((f32[2,2,512]{2,1,0:T(2,128)S(1)}, f32[2,2,512]{2,1,0:T(2,128)S(1)}, f32[2,2,512,128]{3,2,1,0:T(8,128)S(1)})) conditional(s32[]{:T(128)} %convert_element_type.153, (f32[2,2,512]{2,1,0:T(2,128)S(1)}, f32[2,2,512]{2,1,0:T(2,128)S(1)}, f32[2,2,512,128]{3,2,1,0:T(8,128)S(1)}) %tuple.89, (s32[]{:T(128)}, s32[]{:T(128)}, ...), branch_computations={%region_4.4_spmd, %region_5.7_spmd} | conditional | flops 417076224 | bytes 16657448 | solution.py:158
  397.1 6.3 %all-to-all-done.2 = bf16[4,128,512]{2,1,0:T(8,128)(2,1)S(1)} async-done(((bf16[4,128,512]{2,1,0:T(8,128)(2,1)}), bf16[4,128,512]{2,1,0:T(8,128)(2,1)S(1)}, u32[]{:S(2)}, u32[]{:S(2)}) %all-to-all-start.2) | async-done | bytes 524320 | tf_op jit(solution)/shard_map/all_to_all | solution.py:198
  (413 shorter events, 340.9 us)
Async XLA Ops:
  7.2 33.3 %copy-start = (bf16[2048,256]{1,0:T(8,128)(2,1)S(1)}, bf16[2048,256]{1,0:T(8,128)(2,1)}, u32[]{:S(2)}) copy-start(bf16[2048,256]{1,0:T(8,128)(2,1)} %param.20) | copy-start | bytes 3145732
  7.2 32.7 %copy-start.4 = (f32[2048]{0:T(1024)S(1)}, f32[2048]{0:T(1024)}, u32[]{:S(2)}) copy-start(f32[2048]{0:T(1024)} %param.19) | copy-start | bytes 24580
  9.9 29.5 %all-to-all-start = ((bf16[4,128,2048]{2,1,0:T(8,128)(2,1)}), bf16[4,128,2048]{2,1,0:T(8,128)(2,1)S(1)}, u32[]{:S(2)}, u32[]{:S(2)}) async-start(bf16[4,128,2048]{2,1,0:T(8,128)(2,1)} %broadcast_in_dim.44), calls=%async_computation | async-start | bytes 4194304 | tf_op jit(solution)/shard_map/all_to_all | solution.py:16
  13.9 86.9 %all-gather.3.cloned.1.call-start = ((), (), s32[]{:S(2)}) async-start(), calls=%async_computation.3 | async-start | bytes 8650752 | tf_op jit(solution)/shard_map/all_gather | solution.py:122
  39.9 1.4 copy-start.10
  40.5 1.8 copy-start.2
  40.5 1.6 copy-start.7
  42.3 5.5 %copy-start.3 = (bf16[512,2048]{1,0:T(8,128)(2,1)S(1)}, bf16[512,2048]{1,0:T(8,128)(2,1)}, u32[]{:S(2)}) copy-start(bf16[512,2048]{1,0:T(8,128)(2,1)} %copy-done.2) | copy-start | bytes 6291460
  43.2 112.4 %all-gather.5.cloned.1.call-start = ((), (), s32[]{:S(2)}) async-start(), calls=%async_computation.4 | async-start | bytes 8650752 | tf_op jit(solution)/shard_map/all_gather | solution.py:123
  46.7 3.0 copy-start.11
  50.5 4.4 %collective-permute-start = (bf16[30,256]{1,0:T(8,128)(2,1)S(1)}, bf16[30,256]{1,0:T(8,128)(2,1)S(1)}, u32[]{:S(2)}, u32[]{:S(2)}) collective-permute-start(bf16[30,256]{1,0:T(8,128)(2,1)S(1)} %slice.297), channel_id=1, source_target_pairs={{0,4},{4,8},{8,12},{12,16},{16,20},{20,24},{24,28},{28,32},{32,36}... | collective-permute-start | bytes 46088 | tf_op jit(solution)/shard_map/ppermute | solution.py:26
  54.9 10.6 %copy-start.5 = (f32[256]{0:T(256)S(1)}, f32[256]{0:T(256)}, u32[]{:S(2)}) copy-start(f32[256]{0:T(256)} %param.30) | copy-start | bytes 3076
  55.0 10.6 %copy-start.6 = (f32[256]{0:T(256)S(1)}, f32[256]{0:T(256)}, u32[]{:S(2)}) copy-start(f32[256]{0:T(256)} %param.29) | copy-start | bytes 3076
  58.0 7.5 %all-to-all-start.1 = ((f32[4,1,1024]{2,1,0:T(1,128)}), f32[4,1,1024]{2,1,0:T(1,128)S(1)}, u32[]{:S(2)}, u32[]{:S(2)}) async-start(f32[4,1,1024]{2,1,0:T(1,128)} %broadcast_in_dim.45), calls=%async_computation.1 | async-start | bytes 32768 | tf_op jit(solution)/shard_map/all_to_all | solution.py:16
  163.4 227.1 %copy-start.8 = (f32[2]{0:T(128)S(1)}, f32[2]{0:T(128)}, u32[]{:S(2)}) copy-start(f32[2]{0:T(128)} %param.26) | copy-start | bytes 28
  163.4 227.6 %copy-start.9 = (f32[128]{0:T(128)S(1)}, f32[128]{0:T(128)}, u32[]{:S(2)}) copy-start(f32[128]{0:T(128)} %param.27) | copy-start | bytes 1540
  392.5 10.9 %all-to-all-start.2 = ((bf16[4,128,512]{2,1,0:T(8,128)(2,1)}), bf16[4,128,512]{2,1,0:T(8,128)(2,1)S(1)}, u32[]{:S(2)}, u32[]{:S(2)}) async-start(bf16[4,128,512]{2,1,0:T(8,128)(2,1)} %pad_maximum_fusion), calls=%async_computation.2 | async-start | bytes 1048576 | tf_op jit(solution)/shard_map/all_to_all | solution.py:198
  403.7 5.6 %copy-start.1 = (bf16[2048,256]{1,0:T(8,128)(2,1)S(1)}, bf16[2048,256]{1,0:T(8,128)(2,1)}, u32[]{:S(2)}) copy-start(bf16[2048,256]{1,0:T(8,128)(2,1)} %param.20) | copy-start | bytes 3145732
Sparse Core Ops, SparseCore 0:
  43.3 57.4 all-gather.2
  103.2 52.4 all-gather.4
where the time goes:
time: 419 us; the launch traced here: 416 us
  matrix products  159 us (38%)
  waiting for transfers between devices  120 us (29%)
  other arithmetic  48.7 us (12%)
  local copies, waits for them, and re-layouts  40.6 us (10%)
  loops' own time  21 us (5%)
  between operations  14.4 us (3%)
  starting transfers between devices  12.7 us (3%)
    dot_general x32, matrix products, compute(): jnp.einsum('hmqk,khd->hmqd', probs.astype(jnp.bfloat16), value_block, pre...  87.2 us
    dot_general x32, matrix products, compute(): jnp.einsum('hmqd,khmd->hmqk', rq, key_block, preferred_element_type=jnp.f...  59.5 us
    all_gather x1, waiting for transfers between devices, per_device(): value_piece = lax.all_gather(values, 'sp', axis=0, tiled=True)  46.9 us
    all_gather x1, waiting for transfers between devices, per_device(): key_piece = lax.all_gather(rk, 'sp', axis=0, tiled=True)  35.1 us
    reduce_sum x32, other arithmetic, compute(): totals = totals * factor + jnp.sum(probs, axis=-1)  33.3 us
    all_to_all x2, waiting for transfers between devices, sent_to_all(): return lax.all_to_all(copies, axis, split_axis=0, concat_axis=0, tiled=True)  29.2 us
    another operation x1, loops' own time, per_device(): lax.scan(advance, carry, (key_blocks, value_blocks, jnp.arange(blocks, dt...  18.9 us
    dynamic_slice x32, local copies, waits for them, and re-layouts, per_device(): lax.scan(advance, carry, (key_blocks, value_blocks, jnp.arange(blocks, dt...  17.8 us
  transfers between devices with their start and end apart: 6, of which 6 were waited for; matrix products, arithmetic and copies ran while one was open for 5% of the time, Pallas kernels for 0%

commit v1 on v0

--- a/solution.py
+++ b/solution.py
@@ -119,7 +119,9 @@
         jnp.zeros((heads_here, 2, tok_rows, value_size), jnp.float32),
     )
     carry = initial
-    key_piece = lax.all_gather(rk, "sp", axis=0, tiled=True)
+    size = lax.axis_size("sp")
+    repeats = [size if d == 0 else 1 for d in range(rk.ndim)]
+    key_piece = lax.all_to_all(jnp.tile(rk, repeats), "sp", split_axis=0, concat_axis=0, tiled=True)
     value_piece = lax.all_gather(values, "sp", axis=0, tiled=True)
     count = key_piece.shape[0]
     block = math.gcd(count, 512)

time: 419 us -> 541 us (1.29)
  local copies, waits for them, and re-layouts: 40.6 us -> 136 us
  blocking collectives: 0 us -> 29.3 us
  waiting for transfers between devices: 120 us -> 109 us
  starting transfers between devices: 12.7 us -> 18.5 us
    all_to_all x0 -> x1, waiting for transfers between devices: none -> 101 us  [per_device(): lax.all_to_all(jnp.tile(rk, repeats), 'sp', split_axis=0, concat_axis=0,...]
    unnamed x27 -> x30, local copies, waits for them, and re-layouts: 7.7 us -> 96.3 us
    all_gather x1, waiting for transfers between devices: 46.9 us -> 0.01 us  [per_device(): value_piece = lax.all_gather(values, 'sp', axis=0, tiled=True)]
    all_gather x1 -> x0, waiting for transfers between devices: 35.1 us -> none  [per_device(): key_piece = lax.all_gather(rk, 'sp', axis=0, tiled=True)]
    all_to_all x0 -> x1, blocking collectives: none -> 29.3 us  [sent_to_all(): return lax.all_to_all(copies, axis, split_axis=0, concat_axis=0, tiled=True)]
    all_to_all x2 -> x1, waiting for transfers between devices: 29.2 us -> 0.01 us  [sent_to_all(): return lax.all_to_all(copies, axis, split_axis=0, concat_axis=0, tiled=True)]
    another operation x0 -> x1, local copies, waits for them, and re-layouts: none -> 16.4 us  [per_device(): jnp.tile(rk, repeats)]
    all_to_all x0 -> x1, starting transfers between devices: none -> 9.34 us  [per_device(): lax.all_to_all(jnp.tile(rk, repeats), 'sp', split_axis=0, concat_axis=0,...]
  transfers between devices with their start and end apart: 6 -> 5, of which waited for: 6 -> 3; matrix products, arithmetic and copies ran while one was open for 5% -> 21% of each run, Pallas kernels for 0% -> 0%
where the time goes in v1:
time: 541 us; the launch traced here: 536 us
  matrix products  157 us (29%)
  local copies, waits for them, and re-layouts  136 us (25%)
  waiting for transfers between devices  109 us (20%)
  other arithmetic  48 us (9%)
  blocking collectives  29.3 us (5%)
  loops' own time  24 us (4%)
  starting transfers between devices  18.5 us (3%)
  between operations  14.5 us (3%)
    all_to_all x1, waiting for transfers between devices, per_device(): lax.all_to_all(jnp.tile(rk, repeats), 'sp', split_axis=0, concat_axis=0,...  101 us
    unnamed x30, local copies, waits for them, and re-layouts  96.3 us
    dot_general x32, matrix products, compute(): jnp.einsum('hmqk,khd->hmqd', probs.astype(jnp.bfloat16), value_block, pre...  87.2 us
    dot_general x32, matrix products, compute(): jnp.einsum('hmqd,khmd->hmqk', rq, key_block, preferred_element_type=jnp.f...  59.5 us
    reduce_sum x32, other arithmetic, compute(): totals = totals * factor + jnp.sum(probs, axis=-1)  33.3 us
    all_to_all x1, blocking collectives, sent_to_all(): return lax.all_to_all(copies, axis, split_axis=0, concat_axis=0, tiled=True)  29.3 us
    another operation x1, loops' own time, per_device(): lax.scan(advance, carry, (key_blocks, value_blocks, jnp.arange(blocks, dt...  22.1 us
    dynamic_slice x32, local copies, waits for them, and re-layouts, per_device(): lax.scan(advance, carry, (key_blocks, value_blocks, jnp.arange(blocks, dt...  18.8 us
  transfers between devices with their start and end apart: 5, of which 3 were waited for; matrix products, arithmetic and copies ran while one was open for 21% of the time, Pallas kernels for 0%

profile of v1, /device:TPU:121, one launch (start us, length us, event | category | flops | bytes accessed | tf_op | source)
XLA Modules:
  0.0 535.9 jit_solution(15594784260061265112)
XLA Ops:
  8.6 29.3 %all_to_all.29 = bf16[4,128,2048]{2,1,0:T(8,128)(2,1)S(1)} all-to-all(bf16[4,128,2048]{2,1,0:T(8,128)(2,1)S(1)} %broadcast_in_dim.44), channel_id=1, replica_groups=mesh['sp'=32,'tp'=4] {'tp'}, dimensions={0} | all-to-all | bytes 4194304 | tf_op jit(solution)/shard_map/all_to_all | solution.py:16
  55.0 16.4 %tile.4 = bf16[32,512,2,2,64]{4,3,2,1,0:T(2,128)(2,1)} broadcast(bf16[512,2,2,64]{3,2,1,0:T(2,128)(2,1)S(1)} %copy.56), dimensions={1,2,3,4} | broadcast | bytes 8650752 | tf_op jit(solution)/shard_map/tile | solution.py:124
  71.4 26.9 %reshape.216 = bf16[32,2,65536]{2,1,0:T(2,128)(2,1)} reshape(bf16[16384,2,2,64]{3,2,1,0:T(2,128)(2,1)} %bitcast.127) | data formatting | bytes 16777216
  98.3 9.3 %all-to-all-start.1 = ((bf16[32,2,65536]{2,1,0:T(2,128)(2,1)}), bf16[32,2,65536]{2,1,0:T(2,128)(2,1)}, u32[]{:S(2)}, u32[]{:S(2)}) async-start(bf16[32,2,65536]{2,1,0:T(2,128)(2,1)} %reshape.216), calls=%async_computation.1 | async-start | bytes 16777216 | tf_op jit(solution)/shard_map/all_to_all | solution.py:124
  108.0 101.2 %all-to-all-done.1 = bf16[32,2,65536]{2,1,0:T(2,128)(2,1)} async-done(((bf16[32,2,65536]{2,1,0:T(2,128)(2,1)}), bf16[32,2,65536]{2,1,0:T(2,128)(2,1)}, u32[]{:S(2)}, u32[]{:S(2)}) %all-to-all-start.1) | async-done | bytes 8388640 | tf_op jit(solution)/shard_map/all_to_all | solution.py:124
  209.2 26.0 %reshape.217 = bf16[16384,2,2,64]{3,2,1,0:T(2,128)(2,1)} reshape(bf16[32,2,65536]{2,1,0:T(2,128)(2,1)} %all-to-all-done.1) | data formatting | bytes 16777216
  235.3 35.6 %copy.59 = bf16[32,512,2,2,64]{1,4,3,2,0:T(8,128)(2,1)} copy(bf16[32,512,2,2,64]{4,3,2,1,0:T(2,128)(2,1)} %bitcast.126) | data formatting | bytes 16777216
  270.9 7.6 %copy.60 = bf16[32,512,2,128]{3,1,2,0:T(8,128)(2,1)} copy(bf16[32,512,2,128]{3,1,0,2:T(8,128)(2,1)} %bitcast.129) | data formatting | bytes 16777216
  278.6 231.0 %while.15 = (s32[]{:T(128)}, f32[2,2,512]{2,1,0:T(2,128)S(1)}, f32[2,2,512]{2,1,0:T(2,128)S(1)}, f32[2,2,512,128]{3,2,1,0:T(8,128)S(1)}, s32[32]{0:T(128)S(1)}, ...) while((s32[]{:T(128)}, f32[2,2,512]{2,1,0:T(2,128)S(1)}, ...), condition=%wide.region_8.9_spmd.clone, body=%wide.region_3.8_spmd.clone.sunk | while | flops 417076224 | bytes 16659755 | solution.py:162
  279.8 5.9 %conditional.3 = ((f32[2,2,512]{2,1,0:T(2,128)S(1)}, f32[2,2,512]{2,1,0:T(2,128)S(1)}, f32[2,2,512,128]{3,2,1,0:T(8,128)S(1)})) conditional(s32[]{:T(128)} %convert_element_type.157, (f32[2,2,512]{2,1,0:T(2,128)S(1)}, f32[2,2,512]{2,1,0:T(2,128)S(1)}, f32[2,2,512,128]{3,2,1,0:T(8,128)S(1)}) %tuple.90, (s32[]{:T(128)}, s32[]{:T(128)}, ...), branch_computations={%region_4.4_spmd, %region_5.7_spmd} | conditional | flops 417076224 | bytes 16657448 | solution.py:160
  287.1 5.9 %conditional.3 = ((f32[2,2,512]{2,1,0:T(2,128)S(1)}, f32[2,2,512]{2,1,0:T(2,128)S(1)}, f32[2,2,512,128]{3,2,1,0:T(8,128)S(1)})) conditional(s32[]{:T(128)} %convert_element_type.157, (f32[2,2,512]{2,1,0:T(2,128)S(1)}, f32[2,2,512]{2,1,0:T(2,128)S(1)}, f32[2,2,512,128]{3,2,1,0:T(8,128)S(1)}) %tuple.90, (s32[]{:T(128)}, s32[]{:T(128)}, ...), branch_computations={%region_4.4_spmd, %region_5.7_spmd} | conditional | flops 417076224 | bytes 16657448 | solution.py:160
  308.7 5.9 %conditional.3 = ((f32[2,2,512]{2,1,0:T(2,128)S(1)}, f32[2,2,512]{2,1,0:T(2,128)S(1)}, f32[2,2,512,128]{3,2,1,0:T(8,128)S(1)})) conditional(s32[]{:T(128)} %convert_element_type.157, (f32[2,2,512]{2,1,0:T(2,128)S(1)}, f32[2,2,512]{2,1,0:T(2,128)S(1)}, f32[2,2,512,128]{3,2,1,0:T(8,128)S(1)}) %tuple.90, (s32[]{:T(128)}, s32[]{:T(128)}, ...), branch_computations={%region_4.4_spmd, %region_5.7_spmd} | conditional | flops 417076224 | bytes 16657448 | solution.py:160
  330.4 5.9 %conditional.3 = ((f32[2,2,512]{2,1,0:T(2,128)S(1)}, f32[2,2,512]{2,1,0:T(2,128)S(1)}, f32[2,2,512,128]{3,2,1,0:T(8,128)S(1)})) conditional(s32[]{:T(128)} %convert_element_type.157, (f32[2,2,512]{2,1,0:T(2,128)S(1)}, f32[2,2,512]{2,1,0:T(2,128)S(1)}, f32[2,2,512,128]{3,2,1,0:T(8,128)S(1)}) %tuple.90, (s32[]{:T(128)}, s32[]{:T(128)}, ...), branch_computations={%region_4.4_spmd, %region_5.7_spmd} | conditional | flops 417076224 | bytes 16657448 | solution.py:160
  337.6 5.9 %conditional.3 = ((f32[2,2,512]{2,1,0:T(2,128)S(1)}, f32[2,2,512]{2,1,0:T(2,128)S(1)}, f32[2,2,512,128]{3,2,1,0:T(8,128)S(1)})) conditional(s32[]{:T(128)} %convert_element_type.157, (f32[2,2,512]{2,1,0:T(2,128)S(1)}, f32[2,2,512]{2,1,0:T(2,128)S(1)}, f32[2,2,512,128]{3,2,1,0:T(8,128)S(1)}) %tuple.90, (s32[]{:T(128)}, s32[]{:T(128)}, ...), branch_computations={%region_4.4_spmd, %region_5.7_spmd} | conditional | flops 417076224 | bytes 16657448 | solution.py:160
  352.0 5.9 %conditional.3 = ((f32[2,2,512]{2,1,0:T(2,128)S(1)}, f32[2,2,512]{2,1,0:T(2,128)S(1)}, f32[2,2,512,128]{3,2,1,0:T(8,128)S(1)})) conditional(s32[]{:T(128)} %convert_element_type.157, (f32[2,2,512]{2,1,0:T(2,128)S(1)}, f32[2,2,512]{2,1,0:T(2,128)S(1)}, f32[2,2,512,128]{3,2,1,0:T(8,128)S(1)}) %tuple.90, (s32[]{:T(128)}, s32[]{:T(128)}, ...), branch_computations={%region_4.4_spmd, %region_5.7_spmd} | conditional | flops 417076224 | bytes 16657448 | solution.py:160
  373.7 5.9 %conditional.3 = ((f32[2,2,512]{2,1,0:T(2,128)S(1)}, f32[2,2,512]{2,1,0:T(2,128)S(1)}, f32[2,2,512,128]{3,2,1,0:T(8,128)S(1)})) conditional(s32[]{:T(128)} %convert_element_type.157, (f32[2,2,512]{2,1,0:T(2,128)S(1)}, f32[2,2,512]{2,1,0:T(2,128)S(1)}, f32[2,2,512,128]{3,2,1,0:T(8,128)S(1)}) %tuple.90, (s32[]{:T(128)}, s32[]{:T(128)}, ...), branch_computations={%region_4.4_spmd, %region_5.7_spmd} | conditional | flops 417076224 | bytes 16657448 | solution.py:160
  395.4 5.9 %conditional.3 = ((f32[2,2,512]{2,1,0:T(2,128)S(1)}, f32[2,2,512]{2,1,0:T(2,128)S(1)}, f32[2,2,512,128]{3,2,1,0:T(8,128)S(1)})) conditional(s32[]{:T(128)} %convert_element_type.157, (f32[2,2,512]{2,1,0:T(2,128)S(1)}, f32[2,2,512]{2,1,0:T(2,128)S(1)}, f32[2,2,512,128]{3,2,1,0:T(8,128)S(1)}) %tuple.90, (s32[]{:T(128)}, s32[]{:T(128)}, ...), branch_computations={%region_4.4_spmd, %region_5.7_spmd} | conditional | flops 417076224 | bytes 16657448 | solution.py:160
  402.6 5.9 %conditional.3 = ((f32[2,2,512]{2,1,0:T(2,128)S(1)}, f32[2,2,512]{2,1,0:T(2,128)S(1)}, f32[2,2,512,128]{3,2,1,0:T(8,128)S(1)})) conditional(s32[]{:T(128)} %convert_element_type.157, (f32[2,2,512]{2,1,0:T(2,128)S(1)}, f32[2,2,512]{2,1,0:T(2,128)S(1)}, f32[2,2,512,128]{3,2,1,0:T(8,128)S(1)}) %tuple.90, (s32[]{:T(128)}, s32[]{:T(128)}, ...), branch_computations={%region_4.4_spmd, %region_5.7_spmd} | conditional | flops 417076224 | bytes 16657448 | solution.py:160
  417.0 5.9 %conditional.3 = ((f32[2,2,512]{2,1,0:T(2,128)S(1)}, f32[2,2,512]{2,1,0:T(2,128)S(1)}, f32[2,2,512,128]{3,2,1,0:T(8,128)S(1)})) conditional(s32[]{:T(128)} %convert_element_type.157, (f32[2,2,512]{2,1,0:T(2,128)S(1)}, f32[2,2,512]{2,1,0:T(2,128)S(1)}, f32[2,2,512,128]{3,2,1,0:T(8,128)S(1)}) %tuple.90, (s32[]{:T(128)}, s32[]{:T(128)}, ...), branch_computations={%region_4.4_spmd, %region_5.7_spmd} | conditional | flops 417076224 | bytes 16657448 | solution.py:160
  438.7 5.9 %conditional.3 = ((f32[2,2,512]{2,1,0:T(2,128)S(1)}, f32[2,2,512]{2,1,0:T(2,128)S(1)}, f32[2,2,512,128]{3,2,1,0:T(8,128)S(1)})) conditional(s32[]{:T(128)} %convert_element_type.157, (f32[2,2,512]{2,1,0:T(2,128)S(1)}, f32[2,2,512]{2,1,0:T(2,128)S(1)}, f32[2,2,512,128]{3,2,1,0:T(8,128)S(1)}) %tuple.90, (s32[]{:T(128)}, s32[]{:T(128)}, ...), branch_computations={%region_4.4_spmd, %region_5.7_spmd} | conditional | flops 417076224 | bytes 16657448 | solution.py:160
  460.3 5.9 %conditional.3 = ((f32[2,2,512]{2,1,0:T(2,128)S(1)}, f32[2,2,512]{2,1,0:T(2,128)S(1)}, f32[2,2,512,128]{3,2,1,0:T(8,128)S(1)})) conditional(s32[]{:T(128)} %convert_element_type.157, (f32[2,2,512]{2,1,0:T(2,128)S(1)}, f32[2,2,512]{2,1,0:T(2,128)S(1)}, f32[2,2,512,128]{3,2,1,0:T(8,128)S(1)}) %tuple.90, (s32[]{:T(128)}, s32[]{:T(128)}, ...), branch_computations={%region_4.4_spmd, %region_5.7_spmd} | conditional | flops 417076224 | bytes 16657448 | solution.py:160
  482.0 5.9 %conditional.3 = ((f32[2,2,512]{2,1,0:T(2,128)S(1)}, f32[2,2,512]{2,1,0:T(2,128)S(1)}, f32[2,2,512,128]{3,2,1,0:T(8,128)S(1)})) conditional(s32[]{:T(128)} %convert_element_type.157, (f32[2,2,512]{2,1,0:T(2,128)S(1)}, f32[2,2,512]{2,1,0:T(2,128)S(1)}, f32[2,2,512,128]{3,2,1,0:T(8,128)S(1)}) %tuple.90, (s32[]{:T(128)}, s32[]{:T(128)}, ...), branch_computations={%region_4.4_spmd, %region_5.7_spmd} | conditional | flops 417076224 | bytes 16657448 | solution.py:160
  503.7 5.9 %conditional.3 = ((f32[2,2,512]{2,1,0:T(2,128)S(1)}, f32[2,2,512]{2,1,0:T(2,128)S(1)}, f32[2,2,512,128]{3,2,1,0:T(8,128)S(1)})) conditional(s32[]{:T(128)} %convert_element_type.157, (f32[2,2,512]{2,1,0:T(2,128)S(1)}, f32[2,2,512]{2,1,0:T(2,128)S(1)}, f32[2,2,512,128]{3,2,1,0:T(8,128)S(1)}) %tuple.90, (s32[]{:T(128)}, s32[]{:T(128)}, ...), branch_computations={%region_4.4_spmd, %region_5.7_spmd} | conditional | flops 417076224 | bytes 16657448 | solution.py:160
  516.9 6.3 %all-to-all-done.3 = bf16[4,128,512]{2,1,0:T(8,128)(2,1)S(1)} async-done(((bf16[4,128,512]{2,1,0:T(8,128)(2,1)}), bf16[4,128,512]{2,1,0:T(8,128)(2,1)S(1)}, u32[]{:S(2)}, u32[]{:S(2)}) %all-to-all-start.3) | async-done | bytes 524320 | tf_op jit(solution)/shard_map/all_to_all | solution.py:200
  (415 shorter events, 345.6 us)
Async XLA Ops:
  7.2 38.0 %copy-start = (bf16[2048,256]{1,0:T(8,128)(2,1)S(1)}, bf16[2048,256]{1,0:T(8,128)(2,1)}, u32[]{:S(2)}) copy-start(bf16[2048,256]{1,0:T(8,128)(2,1)} %param.20) | copy-start | bytes 3145732
  7.2 31.2 %copy-start.3 = (f32[2048]{0:T(1024)S(1)}, f32[2048]{0:T(1024)}, u32[]{:S(2)}) copy-start(f32[2048]{0:T(1024)} %param.19) | copy-start | bytes 24580
  7.2 263.7 %all-gather.2.cloned.1.call-start = ((), (), s32[]{:S(2)}) async-start(), calls=%async_computation.4 | async-start | bytes 8650752 | tf_op jit(solution)/shard_map/all_gather | solution.py:125
  37.9 1.2 copy-start.9
  38.4 2.4 copy-start.2
  40.8 2.4 copy-start.10
  43.1 2.8 copy-start.11
  43.9 2.9 copy-start.6
  43.9 4.4 collective-permute-start
  51.3 47.0 %all-to-all-start.2 = ((f32[4,1,1024]{2,1,0:T(1,128)}), f32[4,1,1024]{2,1,0:T(1,128)S(1)}, u32[]{:S(2)}, u32[]{:S(2)}) async-start(f32[4,1,1024]{2,1,0:T(1,128)} %broadcast_in_dim.45), calls=%async_computation.2 | async-start | bytes 32768 | tf_op jit(solution)/shard_map/all_to_all | solution.py:16
  98.3 9.4 %copy-start.4 = (f32[256]{0:T(256)S(1)}, f32[256]{0:T(256)}, u32[]{:S(2)}) copy-start(f32[256]{0:T(256)} %param.30) | copy-start | bytes 3076
  98.3 9.4 %copy-start.5 = (f32[256]{0:T(256)S(1)}, f32[256]{0:T(256)}, u32[]{:S(2)}) copy-start(f32[256]{0:T(256)} %param.29) | copy-start | bytes 3076
  98.3 110.9 %all-to-all-start.1 = ((bf16[32,2,65536]{2,1,0:T(2,128)(2,1)}), bf16[32,2,65536]{2,1,0:T(2,128)(2,1)}, u32[]{:S(2)}, u32[]{:S(2)}) async-start(bf16[32,2,65536]{2,1,0:T(2,128)(2,1)} %reshape.216), calls=%async_computation.1 | async-start | bytes 16777216 | tf_op jit(solution)/shard_map/all_to_all | solution.py:124
  278.6 231.1 %copy-start.7 = (f32[2]{0:T(128)S(1)}, f32[2]{0:T(128)}, u32[]{:S(2)}) copy-start(f32[2]{0:T(128)} %param.26) | copy-start | bytes 28
  278.6 231.6 %copy-start.8 = (f32[128]{0:T(128)S(1)}, f32[128]{0:T(128)}, u32[]{:S(2)}) copy-start(f32[128]{0:T(128)} %param.27) | copy-start | bytes 1540
  511.7 11.5 %all-to-all-start.3 = ((bf16[4,128,512]{2,1,0:T(8,128)(2,1)}), bf16[4,128,512]{2,1,0:T(8,128)(2,1)S(1)}, u32[]{:S(2)}, u32[]{:S(2)}) async-start(bf16[4,128,512]{2,1,0:T(8,128)(2,1)} %pad_maximum_fusion), calls=%async_computation.3 | async-start | bytes 1048576 | tf_op jit(solution)/shard_map/all_to_all | solution.py:200
  523.5 5.6 %copy-start.1 = (bf16[2048,256]{1,0:T(8,128)(2,1)S(1)}, bf16[2048,256]{1,0:T(8,128)(2,1)}, u32[]{:S(2)}) copy-start(bf16[2048,256]{1,0:T(8,128)(2,1)} %param.20) | copy-start | bytes 3145732
Sparse Core Ops, SparseCore 0:
  40.9 51.3 all-gather.1
